TPU v7x, 32 devices: a whole 2x2x4 slice. The times are simulated.
32 devices in a mesh: fs: 16 (over z, y, x), tp: 2 (over core).
Axes of the slice: x: 2, y: 2, z: 4, core: 2. Of those that a mesh axis runs over, the one named last changes fastest.
Arguments:
- tokens: bfloat16 [2048, 2048], P('fs', 'tp'), may hold values from -300 to 300
- norm_gain: float32 [2048], P('fs'), may hold values from 0.1 to 1.9
- gate_weight: float32 [16, 2048, 1024], P(None, 'fs', 'tp'), may hold values from -1.3258252 to 1.3258252
- up_weight: float32 [16, 2048, 1024], P(None, 'fs', 'tp'), may hold values from -1.3258252 to 1.3258252
- down_weight: float32 [16, 1024, 2048], P(None, 'fs', 'tp'), may hold values from -0.1875 to 0.1875
- routes: int32 [2048, 4], P('fs'), may hold values from 0 to 15, all different within a row; in each aligned block of 128 rows (0 to 127, 128 to 255, ...) at most 64 rows name the same one
- route_weights: float32 [2048, 4], P('fs'), may hold values from 0.05 to 1
Outputs:
- mixed: bfloat16 [2048, 2048], P('fs', 'tp')
- gate_ready: bfloat16 [16, 2048, 1024], P('fs', None, 'tp')
- up_ready: bfloat16 [16, 2048, 1024], P('fs', None, 'tp')
- down_ready: bfloat16 [16, 1024, 2048], P('fs', None, 'tp')
Inputs may be any that keep to these rules, and one draw needn't show every extreme that they name: `routes`: each row names 4 different experts. In each aligned block of 128 rows no expert is named more than 64 times, a bound that some block reaches.
All inputs are finite; a program needn't handle non-finite values.
Results may differ from a plain program's by a relative error of at most 0.0089.
Values may be sent and summed in bfloat16 or wider, within the bound.
No kernel may reach another device: no remote copies, remote signals or barrier semaphores. Data moves between devices by JAX's collectives and lax.ppermute only.
A program may use at most 64 MiB of HBM per device.

v0:
```python
import jax
import jax.numpy as jnp
from jax import lax
from jax.sharding import PartitionSpec as P

epsilon = 1e-05


def activate(gate_pre, up_pre):
    gated = jnp.minimum(gate_pre, 7.0)
    upper = jnp.clip(up_pre, -7.0, 7.0)
    return (upper + 1.0) * gated * jax.nn.sigmoid(1.702 * gated)


def shards(tokens, norm_gain, gate_weight, up_weight, down_weight, routes, route_weights):
    gate_send = (norm_gain[None, :, None] * gate_weight).astype(jnp.bfloat16)
    up_send = (norm_gain[None, :, None] * up_weight).astype(jnp.bfloat16)
    down_send = down_weight.astype(jnp.bfloat16)
    gate_ready, up_ready, down_ready = (
        lax.all_to_all(gate_send, "fs", split_axis=0, concat_axis=1, tiled=True),
        lax.all_to_all(up_send, "fs", split_axis=0, concat_axis=1, tiled=True),
        lax.all_to_all(down_send, "fs", split_axis=0, concat_axis=1, tiled=True),
    )
    experts = gate_weight.shape[0]
    tok_rows = tokens.shape[0]
    top_count = routes.shape[1]
    pairs = tok_rows * top_count
    capacity = 2 * pairs // experts
    chosen = routes.reshape(pairs)
    onehot = (chosen[:, None] == jnp.arange(experts, dtype=jnp.int32)[None, :]).astype(jnp.int32)
    position = jnp.sum(jnp.cumsum(onehot, axis=0) * onehot, axis=1) - 1
    slot_index = chosen * capacity + position
    token_index = jnp.arange(pairs, dtype=jnp.int32) // top_count
    values = tokens.astype(jnp.float32)
    squared = lax.psum(jnp.sum(values * values, axis=1), "tp")
    width = values.shape[1] * lax.axis_size("tp")
    normed = (values * lax.rsqrt(squared / width + epsilon)[:, None]).astype(jnp.bfloat16)
    outbound = jnp.zeros((experts * capacity, normed.shape[1]), jnp.bfloat16)
    outbound = (
        outbound.at[slot_index].set(normed[token_index]).reshape(experts, capacity, normed.shape[1])
    )
    gate_matrix = gate_ready[0]
    up_matrix = up_ready[0]
    down_matrix = down_ready[0]
    arrived = lax.all_to_all(outbound, "fs", split_axis=0, concat_axis=0, tiled=True)
    arrived = lax.all_gather(arrived, "tp", axis=2, tiled=True)
    sources = arrived.shape[0]
    items = arrived.shape[1]
    arrived_rows = arrived.reshape(sources * items, arrived.shape[2])
    gate_pre = jnp.dot(arrived_rows, gate_matrix, preferred_element_type=jnp.float32)
    up_pre = jnp.dot(arrived_rows, up_matrix, preferred_element_type=jnp.float32)
    hidden = activate(gate_pre, up_pre).astype(jnp.bfloat16)
    summed = jnp.dot(
        lax.all_gather(hidden, "tp", axis=1, tiled=True),
        down_matrix,
        preferred_element_type=jnp.float32,
    )
    results = summed.astype(jnp.bfloat16).reshape(sources, items, down_matrix.shape[1])
    returned = lax.all_to_all(results, "fs", split_axis=0, concat_axis=0, tiled=True)
    flat_back = returned.reshape(experts * capacity, returned.shape[2])
    picked = (
        flat_back[slot_index].astype(jnp.float32).reshape(tok_rows, top_count, returned.shape[2])
    )
    mixed = jnp.sum(picked * route_weights[:, :, None], axis=1).astype(jnp.bfloat16)
    return (mixed, gate_ready, up_ready, down_ready)


def solution(mesh):
    placed = (
        P("fs", "tp"),
        P("fs"),
        P(None, "fs", "tp"),
        P(None, "fs", "tp"),
        P(None, "fs", "tp"),
        P("fs", None),
        P("fs", None),
    )
    return jax.shard_map(
        shards,
        mesh=mesh,
        in_specs=placed,
        out_specs=(P("fs", "tp"), P("fs", None, "tp"), P("fs", None, "tp"), P("fs", None, "tp")),
        check_vma=False,
    )
```

profile of v0, /device:TPU:12, one launch (start us, length us, event | category | flops | bytes accessed | tf_op | source)
XLA Modules:
  0.0 313.8 jit_solution(14182321171666740326)
XLA Ops:
  8.9 1.2 reduce-window.6
  10.6 1.1 fusion.3
  11.7 2.5 psum.7
  14.2 1.1 fusion.4
  15.3 7.7 %scatter_custom_fusion = bf16[1024,1024]{1,0:T(8,128)(2,1)} fusion(s32[512]{0:T(512)S(1)} %bitcast.38, bf16[128,1024]{1,0:T(8,128)(2,1)S(1)} %fusion.4, s32[1024]{0:T(1024)S(1)} %pad_clamp_fusion.1, bf16[]{:T(256)} %constant.15.clone.1), kind=kCustom, calls=%fused_computation.8 | custom fusion | bytes 2097154 | tf_op jit(solution)/shard_map/scatter | solution.py:40
  23.0 7.3 %all-to-all-start = ((bf16[16,64,1024]{2,1,0:T(8,128)(2,1)}), bf16[16,64,1024]{2,1,0:T(8,128)(2,1)}, u32[]{:S(2)}, u32[]{:S(2)}) async-start(bf16[16,64,1024]{2,1,0:T(8,128)(2,1)} %bitcast.4), calls=%async_computation | async-start | bytes 4194304 | tf_op jit(solution)/shard_map/all_to_all | solution.py:45
  30.3 6.1 %multiply_convert_fusion = (bf16[16,128,512]{2,1,0:T(8,128)(2,1)}, bf16[16,128,512]{2,1,0:T(8,128)(2,1)S(1)}) fusion(f32[16,128,512]{2,1,0:T(8,128)} %param.9, f32[128]{0:T(128)S(1)} %copy-done.3, f32[16,128,512]{2,1,0:T(8,128)} %param.10), kind=kLoop, calls=%fused_computation.3 | loop fusion | flops 4194304 | bytes 12583424 | tf_op jit(solution)/shard_map/convert_element_type | solution.py:16
  36.4 42.3 %all-to-all-done = bf16[16,64,1024]{2,1,0:T(8,128)(2,1)} async-done(((bf16[16,64,1024]{2,1,0:T(8,128)(2,1)}), bf16[16,64,1024]{2,1,0:T(8,128)(2,1)}, u32[]{:S(2)}, u32[]{:S(2)}) %all-to-all-start) | async-done | bytes 2097184 | tf_op jit(solution)/shard_map/all_to_all | solution.py:45
  78.8 52.0 %all_to_all.46 = bf16[16,128,512]{2,1,0:T(8,128)(2,1)} all-to-all(bf16[16,128,512]{2,1,0:T(8,128)(2,1)S(1)} %get-tuple-element.5), channel_id=1, replica_groups=mesh['fs'=16,'tp'=2] {'fs'}, dimensions={0} | all-to-all | bytes 4194304 | tf_op jit(solution)/shard_map/all_to_all | solution.py:21
  130.8 5.5 %all-to-all-start.2 = ((bf16[16,128,512]{2,1,0:T(8,128)(2,1)}), bf16[16,128,512]{2,1,0:T(8,128)(2,1)}, u32[]{:S(2)}, u32[]{:S(2)}) async-start(bf16[16,128,512]{2,1,0:T(8,128)(2,1)} %get-tuple-element.4), calls=%async_computation.2 | async-start | bytes 4194304 | tf_op jit(solution)/shard_map/all_to_all | solution.py:20
  137.0 3.8 %convert_element_type.42 = bf16[16,64,1024]{2,1,0:T(8,128)(2,1)} convert(f32[16,64,1024]{2,1,0:T(8,128)} %param.11) | non-fusion elementwise | flops 1048576 | bytes 6291456 | tf_op jit(solution)/shard_map/convert_element_type | solution.py:18
  140.8 42.9 %all-to-all-done.2 = bf16[16,128,512]{2,1,0:T(8,128)(2,1)} async-done(((bf16[16,128,512]{2,1,0:T(8,128)(2,1)}), bf16[16,128,512]{2,1,0:T(8,128)(2,1)}, u32[]{:S(2)}, u32[]{:S(2)}) %all-to-all-start.2) | async-done | bytes 2097184 | tf_op jit(solution)/shard_map/all_to_all | solution.py:20
  183.7 4.7 %all-to-all-start.3 = ((bf16[16,64,1024]{2,1,0:T(8,128)(2,1)}), bf16[16,64,1024]{2,1,0:T(8,128)(2,1)}, u32[]{:S(2)}, u32[]{:S(2)}) async-start(bf16[16,64,1024]{2,1,0:T(8,128)(2,1)} %convert_element_type.42), calls=%async_computation.3 | async-start | bytes 4194304 | tf_op jit(solution)/shard_map/all_to_all | solution.py:22
  188.7 4.7 %fusion.8 = f32[1024,512]{1,0:T(8,128)S(1)} fusion(bf16[1024,2048]{1,0:T(8,128)(2,1)} %bitcast.42, bf16[2048,512]{1,0:T(8,128)(2,1)S(1)} %bitcast.35), kind=kOutput, calls=%fused_computation.34 | convolution fusion | flops 2147483648 | bytes 8388608 | tf_op jit(solution)/shard_map/dot_general | solution.py:51
  193.4 5.4 %multiply_convert_fusion.2 = bf16[1024,512]{1,0:T(8,128)(2,1)} fusion(f32[1024,512]{1,0:T(8,128)S(1)} %fusion.8, bf16[1024,2048]{1,0:T(8,128)(2,1)S(1)} %bitcast.43, bf16[2048,512]{1,0:T(8,128)(2,1)} %bitcast.7), kind=kOutput, calls=%fused_computation.6 | convolution fusion | flops 2152726528 | bytes 9437184 | tf_op jit(solution)/shard_map/dot_general | solution.py:50
  198.8 37.4 %all-to-all-done.3 = bf16[16,64,1024]{2,1,0:T(8,128)(2,1)} async-done(((bf16[16,64,1024]{2,1,0:T(8,128)(2,1)}), bf16[16,64,1024]{2,1,0:T(8,128)(2,1)}, u32[]{:S(2)}, u32[]{:S(2)}) %all-to-all-start.3) | async-done | bytes 2097184 | tf_op jit(solution)/shard_map/all_to_all | solution.py:22
  236.2 5.9 %convolution_convert_fusion = bf16[1024,1024]{1,0:T(8,128)(2,1)} fusion(bf16[1024,1024]{1,0:T(8,128)(2,1)} %all-gather.5.cloned.1.call-done, bf16[1024,1024]{1,0:T(8,128)(2,1)} %bitcast.8), kind=kOutput, calls=%fused_computation.7 | convolution fusion | flops 2148532224 | bytes 6291456 | tf_op jit(solution)/shard_map/dot_general | solution.py:53
  242.1 4.8 %all-to-all-start.4 = ((bf16[16,64,1024]{2,1,0:T(8,128)(2,1)}), bf16[16,64,1024]{2,1,0:T(8,128)(2,1)S(1)}, u32[]{:S(2)}, u32[]{:S(2)}) async-start(bf16[16,64,1024]{2,1,0:T(8,128)(2,1)} %bitcast.37), calls=%async_computation.4 | async-start | bytes 4194304 | tf_op jit(solution)/shard_map/all_to_all | solution.py:59
  247.0 47.5 %all-to-all-done.4 = bf16[16,64,1024]{2,1,0:T(8,128)(2,1)S(1)} async-done(((bf16[16,64,1024]{2,1,0:T(8,128)(2,1)}), bf16[16,64,1024]{2,1,0:T(8,128)(2,1)S(1)}, u32[]{:S(2)}, u32[]{:S(2)}) %all-to-all-start.4) | async-done | bytes 2097184 | tf_op jit(solution)/shard_map/all_to_all | solution.py:59
  294.6 2.0 gather_fusion
  297.3 2.1 multiply_reduce_fusion
  299.4 3.2 %copy.22 = bf16[1,2048,512]{2,1,0:T(8,128)(2,1)} copy(bf16[1,2048,512]{2,1,0:T(8,128)(2,1)} %bitcast.11) | data formatting | bytes 4194304
  302.6 1.3 copy.23
  303.9 3.1 copy.24
  (35 shorter events, 4.1 us)
Async XLA Ops:
  23.0 7.3 %copy-start.3 = (f32[128]{0:T(128)S(1)}, f32[128]{0:T(128)}, u32[]{:S(2)}) copy-start(f32[128]{0:T(128)} %param.8) | copy-start | bytes 1540
  23.0 55.8 %all-to-all-start = ((bf16[16,64,1024]{2,1,0:T(8,128)(2,1)}), bf16[16,64,1024]{2,1,0:T(8,128)(2,1)}, u32[]{:S(2)}, u32[]{:S(2)}) async-start(bf16[16,64,1024]{2,1,0:T(8,128)(2,1)} %bitcast.4), calls=%async_computation | async-start | bytes 4194304 | tf_op jit(solution)/shard_map/all_to_all | solution.py:45
  130.8 52.9 %all-to-all-start.2 = ((bf16[16,128,512]{2,1,0:T(8,128)(2,1)}), bf16[16,128,512]{2,1,0:T(8,128)(2,1)}, u32[]{:S(2)}, u32[]{:S(2)}) async-start(bf16[16,128,512]{2,1,0:T(8,128)(2,1)} %get-tuple-element.4), calls=%async_computation.2 | async-start | bytes 4194304 | tf_op jit(solution)/shard_map/all_to_all | solution.py:20
  136.2 52.4 %all-gather.3.cloned.1.call-start = ((), (), s32[]{:S(2)}) async-start(), calls=%async_computation.5 | async-start | bytes 6291456 | tf_op jit(solution)/shard_map/all_gather | solution.py:46
  140.8 47.9 %copy-start = (bf16[16,128,512]{2,1,0:T(8,128)(2,1)S(1)}, bf16[16,128,512]{2,1,0:T(8,128)(2,1)}, u32[]{:S(2)}) copy-start(bf16[16,128,512]{2,1,0:T(8,128)(2,1)} %all_to_all.46) | copy-start | bytes 6291460
  183.7 52.5 %all-to-all-start.3 = ((bf16[16,64,1024]{2,1,0:T(8,128)(2,1)}), bf16[16,64,1024]{2,1,0:T(8,128)(2,1)}, u32[]{:S(2)}, u32[]{:S(2)}) async-start(bf16[16,64,1024]{2,1,0:T(8,128)(2,1)} %convert_element_type.42), calls=%async_computation.3 | async-start | bytes 4194304 | tf_op jit(solution)/shard_map/all_to_all | solution.py:22
  188.4 47.8 %all-gather.5.cloned.1.call-start = ((), (), s32[]{:S(2)}) async-start(), calls=%async_computation.6 | async-start | bytes 3145728 | tf_op jit(solution)/shard_map/all_gather | solution.py:54
  188.7 4.7 %copy-start.4 = (bf16[16,64,2048]{2,1,0:T(8,128)(2,1)S(1)}, bf16[16,64,2048]{2,1,0:T(8,128)(2,1)}, u32[]{:S(2)}) copy-start(bf16[16,64,2048]{2,1,0:T(8,128)(2,1)} %all-gather.3.cloned.1.call-done) | copy-start | bytes 12582916
  242.1 4.8 %copy-start.2 = (f32[128,4]{0,1:T(4,128)S(1)}, f32[128,4]{0,1:T(4,128)}, u32[]{:S(2)}) copy-start(f32[128,4]{0,1:T(4,128)} %param.13) | copy-start | bytes 6148
  242.1 52.5 %all-to-all-start.4 = ((bf16[16,64,1024]{2,1,0:T(8,128)(2,1)}), bf16[16,64,1024]{2,1,0:T(8,128)(2,1)S(1)}, u32[]{:S(2)}, u32[]{:S(2)}) async-start(bf16[16,64,1024]{2,1,0:T(8,128)(2,1)} %bitcast.37), calls=%async_computation.4 | async-start | bytes 4194304 | tf_op jit(solution)/shard_map/all_to_all | solution.py:59
  299.4 3.2 %copy-start.1 = (bf16[16,128,512]{2,1,0:T(8,128)(2,1)S(1)}, bf16[16,128,512]{2,1,0:T(8,128)(2,1)}, u32[]{:S(2)}) copy-start(bf16[16,128,512]{2,1,0:T(8,128)(2,1)} %all_to_all.46) | copy-start | bytes 6291460
Sparse Core Ops, SparseCore 0:
  138.6 14.8 all-gather.2
  198.9 11.6 all-gather.4
where the time goes:
time: 314 us
  waiting for transfers between devices  171 us (54%)
  blocking collectives  54.4 us (17%)
  starting transfers between devices  22.6 us (7%)
  local copies, waits for them, and re-layouts  19.6 us (6%)
  other arithmetic  16.2 us (5%)
  matrix products  16 us (5%)
  between operations  14.2 us (5%)
    all_to_all x1, blocking collectives, shards(): lax.all_to_all(up_send, 'fs', split_axis=0, concat_axis=1, tiled=True)  52 us
    all_to_all x1, waiting for transfers between devices, shards(): lax.all_to_all(results, 'fs', split_axis=0, concat_axis=0, tiled=True)  47.5 us
    all_to_all x1, waiting for transfers between devices, shards(): lax.all_to_all(gate_send, 'fs', split_axis=0, concat_axis=1, tiled=True)  42.9 us
    all_to_all x1, waiting for transfers between devices, shards(): lax.all_to_all(outbound, 'fs', split_axis=0, concat_axis=0, tiled=True)  42.3 us
    all_to_all x1, waiting for transfers between devices, shards(): lax.all_to_all(down_send, 'fs', split_axis=0, concat_axis=1, tiled=True)  37.4 us
    unnamed x15, local copies, waits for them, and re-layouts  8.51 us
    scatter x1, local copies, waits for them, and re-layouts, shards(): outbound.at[slot_index].set(normed[token_index])  7.72 us
    all_to_all x1, starting transfers between devices, shards(): lax.all_to_all(outbound, 'fs', split_axis=0, concat_axis=0, tiled=True)  7.3 us
  transfers between devices with their start and end apart: 6, of which 4 were waited for; matrix products, arithmetic and copies ran while one was open for 6% of the time, Pallas kernels for 0%

commit v1 on v0

--- a/solution.py
+++ b/solution.py
@@ -4,6 +4,29 @@
 from jax.sharding import PartitionSpec as P
 
 epsilon = 1e-05
+
+
+def in_blocks(x, dim, size):
+    shape = x.shape
+    pieces = x.reshape(*shape[:dim], size, shape[dim] // size, *shape[dim + 1 :])
+    return jnp.moveaxis(pieces, dim, 0)
+
+
+def joined_along(parts, dim):
+    parts = jnp.moveaxis(parts, 0, dim)
+    lengths = parts.shape
+    return parts.reshape(*lengths[:dim], lengths[dim] * lengths[dim + 1], *lengths[dim + 2 :])
+
+
+def pairwise_exchange(x, axis, split_dim, concat_dim):
+    size, index = (lax.axis_size(axis), lax.axis_index(axis))
+    tiles = in_blocks(x, split_dim, size)
+    done = [tiles[index]]
+    for step in range(1, size):
+        sent = tiles[index ^ step]
+        done.append(lax.ppermute(sent, axis, [(i, i ^ step) for i in range(size)]))
+    tiles = jnp.stack(done)[index ^ jnp.arange(size)]
+    return joined_along(tiles, concat_dim)
 
 
 def activate(gate_pre, up_pre):
@@ -42,7 +65,7 @@
     gate_matrix = gate_ready[0]
     up_matrix = up_ready[0]
     down_matrix = down_ready[0]
-    arrived = lax.all_to_all(outbound, "fs", split_axis=0, concat_axis=0, tiled=True)
+    arrived = pairwise_exchange(outbound, "fs", 0, 0)
     arrived = lax.all_gather(arrived, "tp", axis=2, tiled=True)
     sources = arrived.shape[0]
     items = arrived.shape[1]

time: 314 us -> 297 us (0.946)
  blocking collectives: 54.4 us -> 2.46 us
  starting transfers between devices: 22.6 us -> 49.7 us
  local copies, waits for them, and re-layouts: 19.6 us -> 35 us
  waiting for transfers between devices: 171 us -> 165 us
    all_to_all x1 -> x0, blocking collectives: 52 us -> none  [shards(): lax.all_to_all(up_send, 'fs', split_axis=0, concat_axis=1, tiled=True)]
    ppermute x0 -> x15, waiting for transfers between devices: none -> 43 us  [pairwise_exchange(): done.append(lax.ppermute(sent, axis, [(i, i ^ step) for i in range(size)]))]
    all_to_all x1, waiting for transfers between devices: 42.3 us -> 0.01 us  [shards(): lax.all_to_all(up_send, 'fs', split_axis=0, concat_axis=1, tiled=True)]
    ppermute x0 -> x15, starting transfers between devices: none -> 25 us  [pairwise_exchange(): done.append(lax.ppermute(sent, axis, [(i, i ^ step) for i in range(size)]))]
    unnamed x15 -> x31, local copies, waits for them, and re-layouts: 8.51 us -> 17.1 us
    all_to_all x1, waiting for transfers between devices: 42.9 us -> 38.2 us  [shards(): lax.all_to_all(gate_send, 'fs', split_axis=0, concat_axis=1, tiled=True)]
    gather x0 -> x1, local copies, waits for them, and re-layouts: none -> 3.59 us  [pairwise_exchange(): tiles = jnp.stack(done)[index ^ jnp.arange(size)]]
  transfers between devices with their start and end apart: 6 -> 21, of which waited for: 4 -> 15; matrix products, arithmetic and copies ran while one was open for 6% -> 14% of each run, Pallas kernels for 0% -> 0%
where the time goes in v1:
time: 297 us
  waiting for transfers between devices  165 us (56%)
  starting transfers between devices  49.7 us (17%)
  local copies, waits for them, and re-layouts  35 us (12%)
  matrix products  15.9 us (5%)
  other arithmetic  14.3 us (5%)
  between operations  14.2 us (5%)
    all_to_all x1, waiting for transfers between devices, shards(): lax.all_to_all(results, 'fs', split_axis=0, concat_axis=0, tiled=True)  47.3 us
    ppermute x15, waiting for transfers between devices, pairwise_exchange(): done.append(lax.ppermute(sent, axis, [(i, i ^ step) for i in range(size)]))  43 us
    all_to_all x1, waiting for transfers between devices, shards(): lax.all_to_all(gate_send, 'fs', split_axis=0, concat_axis=1, tiled=True)  38.2 us
    all_to_all x1, waiting for transfers between devices, shards(): lax.all_to_all(down_send, 'fs', split_axis=0, concat_axis=1, tiled=True)  36.6 us
    ppermute x15, starting transfers between devices, pairwise_exchange(): done.append(lax.ppermute(sent, axis, [(i, i ^ step) for i in range(size)]))  25 us
    unnamed x31, local copies, waits for them, and re-layouts  17.1 us
    scatter x1, local copies, waits for them, and re-layouts, shards(): outbound.at[slot_index].set(normed[token_index])  7.72 us
    all_to_all x1, starting transfers between devices, shards(): lax.all_to_all(up_send, 'fs', split_axis=0, concat_axis=1, tiled=True)  7.3 us
  transfers between devices with their start and end apart: 21, of which 15 were waited for; matrix products, arithmetic and copies ran while one was open for 14% of the time, Pallas kernels for 0%

profile of v1, /device:TPU:12, one launch (start us, length us, event | category | flops | bytes accessed | tf_op | source)
XLA Modules:
  0.0 296.8 jit_solution(18176437071766621119)
XLA Ops:
  7.2 6.8 %multiply_convert_fusion = (bf16[16,128,512]{2,1,0:T(8,128)(2,1)}, bf16[16,128,512]{2,1,0:T(8,128)(2,1)}) fusion(f32[16,128,512]{2,1,0:T(8,128)} %param.9, f32[128]{0:T(128)} %param.8, f32[16,128,512]{2,1,0:T(8,128)} %param.10), kind=kLoop, calls=%fused_computation.4 | loop fusion | flops 4194304 | bytes 12583424 | tf_op jit(solution)/shard_map/convert_element_type | solution.py:39
  14.0 7.3 %all-to-all-start = ((bf16[16,128,512]{2,1,0:T(8,128)(2,1)}), bf16[16,128,512]{2,1,0:T(8,128)(2,1)S(1)}, u32[]{:S(2)}, u32[]{:S(2)}) async-start(bf16[16,128,512]{2,1,0:T(8,128)(2,1)} %get-tuple-element.21), calls=%async_computation | async-start | bytes 4194304 | tf_op jit(solution)/shard_map/all_to_all | solution.py:44
  26.2 7.7 %scatter_custom_fusion = bf16[1024,1024]{1,0:T(8,128)(2,1)} fusion(s32[512]{0:T(512)S(1)} %bitcast.102, bf16[128,1024]{1,0:T(8,128)(2,1)S(1)} %fusion.4, s32[1024]{0:T(1024)S(1)} %pad_clamp_fusion.2, bf16[]{:T(256)} %constant.32.clone.1), kind=kCustom, calls=%fused_computation.9 | custom fusion | bytes 2097154 | tf_op jit(solution)/shard_map/scatter | solution.py:63
  42.8 7.8 %collective-permute-done = bf16[1,64,1024]{2,1,0:T(8,128)(2,1)S(1)} collective-permute-done((bf16[1,64,1024]{2,1,0:T(8,128)(2,1)S(1)}, bf16[1,64,1024]{2,1,0:T(8,128)(2,1)S(1)}, u32[]{:S(2)}, u32[]{:S(2)}) %collective-permute-start) | collective-permute-done | bytes 131104 | tf_op jit(solution)/shard_map/ppermute | solution.py:27
  66.1 3.2 %collective-permute-start.10 = (bf16[1,64,1024]{2,1,0:T(8,128)(2,1)S(1)}, bf16[1,64,1024]{2,1,0:T(8,128)(2,1)S(1)}, u32[]{:S(2)}, u32[]{:S(2)}) collective-permute-start(bf16[1,64,1024]{2,1,0:T(8,128)(2,1)S(1)} %get-tuple-element.8), channel_id=1, source_target_pairs={{0,22},{2,20},{4,18},{6,16},{8,30},{10,28},{12,26},{14,24},{16,6},... | collective-permute-start | bytes 393224 | tf_op jit(solution)/shard_map/ppermute | solution.py:27
  70.4 4.0 %collective-permute-start.11 = (bf16[1,64,1024]{2,1,0:T(8,128)(2,1)S(1)}, bf16[1,64,1024]{2,1,0:T(8,128)(2,1)S(1)}, u32[]{:S(2)}, u32[]{:S(2)}) collective-permute-start(bf16[1,64,1024]{2,1,0:T(8,128)(2,1)S(1)} %get-tuple-element.7), channel_id=1, source_target_pairs={{0,24},{2,26},{4,28},{6,30},{8,16},{10,18},{12,20},{14,22},{16,8},... | collective-permute-start | bytes 393224 | tf_op jit(solution)/shard_map/ppermute | solution.py:27
  75.1 10.6 %collective-permute-done.7 = bf16[1,64,1024]{2,1,0:T(8,128)(2,1)S(1)} collective-permute-done((bf16[1,64,1024]{2,1,0:T(8,128)(2,1)S(1)}, bf16[1,64,1024]{2,1,0:T(8,128)(2,1)S(1)}, u32[]{:S(2)}, u32[]{:S(2)}) %collective-permute-start.7) | collective-permute-done | bytes 131104 | tf_op jit(solution)/shard_map/ppermute | solution.py:27
  85.8 3.0 %collective-permute-start.12 = (bf16[1,64,1024]{2,1,0:T(8,128)(2,1)S(1)}, bf16[1,64,1024]{2,1,0:T(8,128)(2,1)S(1)}, u32[]{:S(2)}, u32[]{:S(2)}) collective-permute-start(bf16[1,64,1024]{2,1,0:T(8,128)(2,1)S(1)} %get-tuple-element.6), channel_id=1, source_target_pairs={{0,26},{2,24},{4,30},{6,28},{8,18},{10,16},{12,22},{14,20},{16,10}... | collective-permute-start | bytes 393224 | tf_op jit(solution)/shard_map/ppermute | solution.py:27
  90.7 4.9 %collective-permute-done.9 = bf16[1,64,1024]{2,1,0:T(8,128)(2,1)S(1)} collective-permute-done((bf16[1,64,1024]{2,1,0:T(8,128)(2,1)S(1)}, bf16[1,64,1024]{2,1,0:T(8,128)(2,1)S(1)}, u32[]{:S(2)}, u32[]{:S(2)}) %collective-permute-start.9) | collective-permute-done | bytes 131104 | tf_op jit(solution)/shard_map/ppermute | solution.py:27
  97.1 4.1 %collective-permute-done.10 = bf16[1,64,1024]{2,1,0:T(8,128)(2,1)S(1)} collective-permute-done((bf16[1,64,1024]{2,1,0:T(8,128)(2,1)S(1)}, bf16[1,64,1024]{2,1,0:T(8,128)(2,1)S(1)}, u32[]{:S(2)}, u32[]{:S(2)}) %collective-permute-start.10) | collective-permute-done | bytes 131104 | tf_op jit(solution)/shard_map/ppermute | solution.py:27
  101.9 7.6 %collective-permute-done.11 = bf16[1,64,1024]{2,1,0:T(8,128)(2,1)S(1)} collective-permute-done((bf16[1,64,1024]{2,1,0:T(8,128)(2,1)S(1)}, bf16[1,64,1024]{2,1,0:T(8,128)(2,1)S(1)}, u32[]{:S(2)}, u32[]{:S(2)}) %collective-permute-start.11) | collective-permute-done | bytes 131104 | tf_op jit(solution)/shard_map/ppermute | solution.py:27
  113.7 6.8 %all-to-all-start.1 = ((bf16[16,128,512]{2,1,0:T(8,128)(2,1)}), bf16[16,128,512]{2,1,0:T(8,128)(2,1)}, u32[]{:S(2)}, u32[]{:S(2)}) async-start(bf16[16,128,512]{2,1,0:T(8,128)(2,1)} %get-tuple-element.20), calls=%async_computation.1 | async-start | bytes 4194304 | tf_op jit(solution)/shard_map/all_to_all | solution.py:43
  121.2 3.6 %gather_fusion = bf16[16,64,1024]{2,1,0:T(8,128)(2,1)} fusion(bf16[16,64,1024]{2,1,0:T(8,128)(2,1)} %bitcast.35, s32[1024]{0:T(1024)S(1)} %pad_clamp_fusion.1), kind=kCustom, calls=%fused_computation.1 | custom fusion | bytes 4194368 | tf_op jit(solution)/shard_map/gather | solution.py:28
  124.9 3.8 %convert_element_type.42 = bf16[16,64,1024]{2,1,0:T(8,128)(2,1)} convert(f32[16,64,1024]{2,1,0:T(8,128)} %param.11) | non-fusion elementwise | flops 1048576 | bytes 6291456 | tf_op jit(solution)/shard_map/convert_element_type | solution.py:41
  128.7 38.2 %all-to-all-done.1 = bf16[16,128,512]{2,1,0:T(8,128)(2,1)} async-done(((bf16[16,128,512]{2,1,0:T(8,128)(2,1)}), bf16[16,128,512]{2,1,0:T(8,128)(2,1)}, u32[]{:S(2)}, u32[]{:S(2)}) %all-to-all-start.1) | async-done | bytes 2097184 | tf_op jit(solution)/shard_map/all_to_all | solution.py:43
  166.8 5.7 %all-to-all-start.2 = ((bf16[16,64,1024]{2,1,0:T(8,128)(2,1)}), bf16[16,64,1024]{2,1,0:T(8,128)(2,1)}, u32[]{:S(2)}, u32[]{:S(2)}) async-start(bf16[16,64,1024]{2,1,0:T(8,128)(2,1)} %convert_element_type.42), calls=%async_computation.2 | async-start | bytes 4194304 | tf_op jit(solution)/shard_map/all_to_all | solution.py:45
  172.6 4.7 %fusion.9 = f32[1024,512]{1,0:T(8,128)S(1)} fusion(bf16[1024,2048]{1,0:T(8,128)(2,1)} %bitcast.106, bf16[2048,512]{1,0:T(8,128)(2,1)S(1)} %bitcast.98), kind=kOutput, calls=%fused_computation.69 | convolution fusion | flops 2147483648 | bytes 8388608 | tf_op jit(solution)/shard_map/dot_general | solution.py:74
  177.3 5.4 %multiply_convert_fusion.2 = bf16[1024,512]{1,0:T(8,128)(2,1)} fusion(f32[1024,512]{1,0:T(8,128)S(1)} %fusion.9, bf16[1024,2048]{1,0:T(8,128)(2,1)S(1)} %bitcast.107, bf16[2048,512]{1,0:T(8,128)(2,1)} %bitcast.39), kind=kOutput, calls=%fused_computation.7 | convolution fusion | flops 2152726528 | bytes 9437184 | tf_op jit(solution)/shard_map/dot_general | solution.py:73
  182.7 36.6 %all-to-all-done.2 = bf16[16,64,1024]{2,1,0:T(8,128)(2,1)} async-done(((bf16[16,64,1024]{2,1,0:T(8,128)(2,1)}), bf16[16,64,1024]{2,1,0:T(8,128)(2,1)}, u32[]{:S(2)}, u32[]{:S(2)}) %all-to-all-start.2) | async-done | bytes 2097184 | tf_op jit(solution)/shard_map/all_to_all | solution.py:45
  219.3 5.9 %convolution_convert_fusion = bf16[1024,1024]{1,0:T(8,128)(2,1)} fusion(bf16[1024,1024]{1,0:T(8,128)(2,1)} %all-gather.4.cloned.1.call-done, bf16[1024,1024]{1,0:T(8,128)(2,1)} %bitcast.40), kind=kOutput, calls=%fused_computation.8 | convolution fusion | flops 2148532224 | bytes 6291456 | tf_op jit(solution)/shard_map/dot_general | solution.py:76
  225.2 4.9 %all-to-all-start.3 = ((bf16[16,64,1024]{2,1,0:T(8,128)(2,1)}), bf16[16,64,1024]{2,1,0:T(8,128)(2,1)S(1)}, u32[]{:S(2)}, u32[]{:S(2)}) async-start(bf16[16,64,1024]{2,1,0:T(8,128)(2,1)} %bitcast.101), calls=%async_computation.3 | async-start | bytes 4194304 | tf_op jit(solution)/shard_map/all_to_all | solution.py:82
  230.2 47.3 %all-to-all-done.3 = bf16[16,64,1024]{2,1,0:T(8,128)(2,1)S(1)} async-done(((bf16[16,64,1024]{2,1,0:T(8,128)(2,1)}), bf16[16,64,1024]{2,1,0:T(8,128)(2,1)S(1)}, u32[]{:S(2)}, u32[]{:S(2)}) %all-to-all-start.3) | async-done | bytes 2097184 | tf_op jit(solution)/shard_map/all_to_all | solution.py:82
  282.3 3.2 %copy.37 = bf16[1,2048,512]{2,1,0:T(8,128)(2,1)} copy(bf16[1,2048,512]{2,1,0:T(8,128)(2,1)} %bitcast.43) | data formatting | bytes 4194304
  286.8 3.1 %copy.39 = bf16[1,1024,1024]{2,1,0:T(8,128)(2,1)} copy(bf16[1,1024,1024]{2,1,0:T(8,128)(2,1)} %bitcast.45) | data formatting | bytes 4194304
  (85 shorter events, 46.4 us)
Async XLA Ops:
  14.0 7.3 %copy-start.3 = (s32[128,4]{0,1:T(4,128)S(1)}, s32[128,4]{0,1:T(4,128)}, u32[]{:S(2)}) copy-start(s32[128,4]{0,1:T(4,128)} %param.12) | copy-start | bytes 6148
  14.0 9.4 %copy-start.2 = (bf16[128,1024]{1,0:T(8,128)(2,1)S(1)}, bf16[128,1024]{1,0:T(8,128)(2,1)}, u32[]{:S(2)}) copy-start(bf16[128,1024]{1,0:T(8,128)(2,1)} %param.7) | copy-start | bytes 786436
  14.0 99.7 %all-to-all-start = ((bf16[16,128,512]{2,1,0:T(8,128)(2,1)}), bf16[16,128,512]{2,1,0:T(8,128)(2,1)S(1)}, u32[]{:S(2)}, u32[]{:S(2)}) async-start(bf16[16,128,512]{2,1,0:T(8,128)(2,1)} %get-tuple-element.21), calls=%async_computation | async-start | bytes 4194304 | tf_op jit(solution)/shard_map/all_to_all | solution.py:44
  36.4 14.2 %collective-permute-start = (bf16[1,64,1024]{2,1,0:T(8,128)(2,1)S(1)}, bf16[1,64,1024]{2,1,0:T(8,128)(2,1)S(1)}, u32[]{:S(2)}, u32[]{:S(2)}) collective-permute-start(bf16[1,64,1024]{2,1,0:T(8,128)(2,1)S(1)} %get-tuple-element.18), channel_id=1, source_target_pairs={{0,2},{2,0},{4,6},{6,4},{8,10},{10,8},{12,14},{14,12},{16,18},{18,... | collective-permute-start | bytes 393224 | tf_op jit(solution)/shard_map/ppermute | solution.py:27
  37.8 15.2 %collective-permute-start.1 = (bf16[1,64,1024]{2,1,0:T(8,128)(2,1)S(1)}, bf16[1,64,1024]{2,1,0:T(8,128)(2,1)S(1)}, u32[]{:S(2)}, u32[]{:S(2)}) collective-permute-start(bf16[1,64,1024]{2,1,0:T(8,128)(2,1)S(1)} %get-tuple-element.17), channel_id=1, source_target_pairs={{0,4},{2,6},{4,0},{6,2},{8,12},{10,14},{12,8},{14,10},{16,20},{18,... | collective-permute-start | bytes 393224 | tf_op jit(solution)/shard_map/ppermute | solution.py:27
  38.4 19.3 %collective-permute-start.2 = (bf16[1,64,1024]{2,1,0:T(8,128)(2,1)S(1)}, bf16[1,64,1024]{2,1,0:T(8,128)(2,1)S(1)}, u32[]{:S(2)}, u32[]{:S(2)}) collective-permute-start(bf16[1,64,1024]{2,1,0:T(8,128)(2,1)S(1)} %get-tuple-element.16), channel_id=1, source_target_pairs={{0,6},{2,4},{4,2},{6,0},{8,14},{10,12},{12,10},{14,8},{16,22},{18,... | collective-permute-start | bytes 393224 | tf_op jit(solution)/shard_map/ppermute | solution.py:27
  39.9 20.6 %collective-permute-start.3 = (bf16[1,64,1024]{2,1,0:T(8,128)(2,1)S(1)}, bf16[1,64,1024]{2,1,0:T(8,128)(2,1)S(1)}, u32[]{:S(2)}, u32[]{:S(2)}) collective-permute-start(bf16[1,64,1024]{2,1,0:T(8,128)(2,1)S(1)} %get-tuple-element.15), channel_id=1, source_target_pairs={{0,8},{2,10},{4,12},{6,14},{8,0},{10,2},{12,4},{14,6},{16,24},{18,... | collective-permute-start | bytes 393224 | tf_op jit(solution)/shard_map/ppermute | solution.py:27
  40.4 23.5 %collective-permute-start.4 = (bf16[1,64,1024]{2,1,0:T(8,128)(2,1)S(1)}, bf16[1,64,1024]{2,1,0:T(8,128)(2,1)S(1)}, u32[]{:S(2)}, u32[]{:S(2)}) collective-permute-start(bf16[1,64,1024]{2,1,0:T(8,128)(2,1)S(1)} %get-tuple-element.14), channel_id=1, source_target_pairs={{0,10},{2,8},{4,14},{6,12},{8,2},{10,0},{12,6},{14,4},{16,26},{18,... | collective-permute-start | bytes 393224 | tf_op jit(solution)/shard_map/ppermute | solution.py:27
  50.6 15.5 %collective-permute-start.5 = (bf16[1,64,1024]{2,1,0:T(8,128)(2,1)S(1)}, bf16[1,64,1024]{2,1,0:T(8,128)(2,1)S(1)}, u32[]{:S(2)}, u32[]{:S(2)}) collective-permute-start(bf16[1,64,1024]{2,1,0:T(8,128)(2,1)S(1)} %get-tuple-element.13), channel_id=1, source_target_pairs={{0,12},{2,14},{4,8},{6,10},{8,4},{10,6},{12,0},{14,2},{16,28},{18,... | collective-permute-start | bytes 393224 | tf_op jit(solution)/shard_map/ppermute | solution.py:27
  53.0 17.4 %collective-permute-start.6 = (bf16[1,64,1024]{2,1,0:T(8,128)(2,1)S(1)}, bf16[1,64,1024]{2,1,0:T(8,128)(2,1)S(1)}, u32[]{:S(2)}, u32[]{:S(2)}) collective-permute-start(bf16[1,64,1024]{2,1,0:T(8,128)(2,1)S(1)} %get-tuple-element.12), channel_id=1, source_target_pairs={{0,14},{2,12},{4,10},{6,8},{8,6},{10,4},{12,2},{14,0},{16,30},{18,... | collective-permute-start | bytes 393224 | tf_op jit(solution)/shard_map/ppermute | solution.py:27
  57.7 28.1 %collective-permute-start.7 = (bf16[1,64,1024]{2,1,0:T(8,128)(2,1)S(1)}, bf16[1,64,1024]{2,1,0:T(8,128)(2,1)S(1)}, u32[]{:S(2)}, u32[]{:S(2)}) collective-permute-start(bf16[1,64,1024]{2,1,0:T(8,128)(2,1)S(1)} %get-tuple-element.11), channel_id=1, source_target_pairs={{0,16},{2,18},{4,20},{6,22},{8,24},{10,26},{12,28},{14,30},{16,0},... | collective-permute-start | bytes 393224 | tf_op jit(solution)/shard_map/ppermute | solution.py:27
  60.4 29.0 %collective-permute-start.8 = (bf16[1,64,1024]{2,1,0:T(8,128)(2,1)S(1)}, bf16[1,64,1024]{2,1,0:T(8,128)(2,1)S(1)}, u32[]{:S(2)}, u32[]{:S(2)}) collective-permute-start(bf16[1,64,1024]{2,1,0:T(8,128)(2,1)S(1)} %get-tuple-element.10), channel_id=1, source_target_pairs={{0,18},{2,16},{4,22},{6,20},{8,26},{10,24},{12,30},{14,28},{16,2},... | collective-permute-start | bytes 393224 | tf_op jit(solution)/shard_map/ppermute | solution.py:27
  64.0 31.6 %collective-permute-start.9 = (bf16[1,64,1024]{2,1,0:T(8,128)(2,1)S(1)}, bf16[1,64,1024]{2,1,0:T(8,128)(2,1)S(1)}, u32[]{:S(2)}, u32[]{:S(2)}) collective-permute-start(bf16[1,64,1024]{2,1,0:T(8,128)(2,1)S(1)} %get-tuple-element.9), channel_id=1, source_target_pairs={{0,20},{2,22},{4,16},{6,18},{8,28},{10,30},{12,24},{14,26},{16,4},... | collective-permute-start | bytes 393224 | tf_op jit(solution)/shard_map/ppermute | solution.py:27
  66.1 35.2 %collective-permute-start.10 = (bf16[1,64,1024]{2,1,0:T(8,128)(2,1)S(1)}, bf16[1,64,1024]{2,1,0:T(8,128)(2,1)S(1)}, u32[]{:S(2)}, u32[]{:S(2)}) collective-permute-start(bf16[1,64,1024]{2,1,0:T(8,128)(2,1)S(1)} %get-tuple-element.8), channel_id=1, source_target_pairs={{0,22},{2,20},{4,18},{6,16},{8,30},{10,28},{12,26},{14,24},{16,6},... | collective-permute-start | bytes 393224 | tf_op jit(solution)/shard_map/ppermute | solution.py:27
  70.4 39.0 %collective-permute-start.11 = (bf16[1,64,1024]{2,1,0:T(8,128)(2,1)S(1)}, bf16[1,64,1024]{2,1,0:T(8,128)(2,1)S(1)}, u32[]{:S(2)}, u32[]{:S(2)}) collective-permute-start(bf16[1,64,1024]{2,1,0:T(8,128)(2,1)S(1)} %get-tuple-element.7), channel_id=1, source_target_pairs={{0,24},{2,26},{4,28},{6,30},{8,16},{10,18},{12,20},{14,22},{16,8},... | collective-permute-start | bytes 393224 | tf_op jit(solution)/shard_map/ppermute | solution.py:27
  85.8 25.9 %collective-permute-start.12 = (bf16[1,64,1024]{2,1,0:T(8,128)(2,1)S(1)}, bf16[1,64,1024]{2,1,0:T(8,128)(2,1)S(1)}, u32[]{:S(2)}, u32[]{:S(2)}) collective-permute-start(bf16[1,64,1024]{2,1,0:T(8,128)(2,1)S(1)} %get-tuple-element.6), channel_id=1, source_target_pairs={{0,26},{2,24},{4,30},{6,28},{8,18},{10,16},{12,22},{14,20},{16,10}... | collective-permute-start | bytes 393224 | tf_op jit(solution)/shard_map/ppermute | solution.py:27
  89.5 23.6 %collective-permute-start.13 = (bf16[1,64,1024]{2,1,0:T(8,128)(2,1)S(1)}, bf16[1,64,1024]{2,1,0:T(8,128)(2,1)S(1)}, u32[]{:S(2)}, u32[]{:S(2)}) collective-permute-start(bf16[1,64,1024]{2,1,0:T(8,128)(2,1)S(1)} %get-tuple-element.5), channel_id=1, source_target_pairs={{0,28},{2,30},{4,24},{6,26},{8,20},{10,22},{12,16},{14,18},{16,12}... | collective-permute-start | bytes 393224 | tf_op jit(solution)/shard_map/ppermute | solution.py:27
  95.6 25.0 %collective-permute-start.14 = (bf16[1,64,1024]{2,1,0:T(8,128)(2,1)S(1)}, bf16[1,64,1024]{2,1,0:T(8,128)(2,1)S(1)}, u32[]{:S(2)}, u32[]{:S(2)}) collective-permute-start(bf16[1,64,1024]{2,1,0:T(8,128)(2,1)S(1)} %get-tuple-element.4), channel_id=1, source_target_pairs={{0,30},{2,28},{4,26},{6,24},{8,22},{10,20},{12,18},{14,16},{16,14}... | collective-permute-start | bytes 393224 | tf_op jit(solution)/shard_map/ppermute | solution.py:27
  113.7 58.8 %copy-start = (bf16[16,128,512]{2,1,0:T(8,128)(2,1)}, bf16[16,128,512]{2,1,0:T(8,128)(2,1)S(1)}, u32[]{:S(2)}) copy-start(bf16[16,128,512]{2,1,0:T(8,128)(2,1)S(1)} %all-to-all-done) | copy-start | bytes 6291460
  113.7 53.1 %all-to-all-start.1 = ((bf16[16,128,512]{2,1,0:T(8,128)(2,1)}), bf16[16,128,512]{2,1,0:T(8,128)(2,1)}, u32[]{:S(2)}, u32[]{:S(2)}) async-start(bf16[16,128,512]{2,1,0:T(8,128)(2,1)} %get-tuple-element.20), calls=%async_computation.1 | async-start | bytes 4194304 | tf_op jit(solution)/shard_map/all_to_all | solution.py:43
  120.5 52.0 %all-gather.6.cloned.1.call-start = ((), (), s32[]{:S(2)}) async-start(), calls=%async_computation.5 | async-start | bytes 6291456 | tf_op jit(solution)/shard_map/all_gather | solution.py:69
  166.8 52.4 %all-to-all-start.2 = ((bf16[16,64,1024]{2,1,0:T(8,128)(2,1)}), bf16[16,64,1024]{2,1,0:T(8,128)(2,1)}, u32[]{:S(2)}, u32[]{:S(2)}) async-start(bf16[16,64,1024]{2,1,0:T(8,128)(2,1)} %convert_element_type.42), calls=%async_computation.2 | async-start | bytes 4194304 | tf_op jit(solution)/shard_map/all_to_all | solution.py:45
  172.5 46.8 %all-gather.4.cloned.1.call-start = ((), (), s32[]{:S(2)}) async-start(), calls=%async_computation.4 | async-start | bytes 3145728 | tf_op jit(solution)/shard_map/all_gather | solution.py:77
  225.2 52.3 %all-to-all-start.3 = ((bf16[16,64,1024]{2,1,0:T(8,128)(2,1)}), bf16[16,64,1024]{2,1,0:T(8,128)(2,1)S(1)}, u32[]{:S(2)}, u32[]{:S(2)}) async-start(bf16[16,64,1024]{2,1,0:T(8,128)(2,1)} %bitcast.101), calls=%async_computation.3 | async-start | bytes 4194304 | tf_op jit(solution)/shard_map/all_to_all | solution.py:82
  (3 other events, 12.8 us)
Sparse Core Ops, SparseCore 0:
  125.0 14.7 all-gather.5
  182.8 11.7 all-gather.3
